TPU v7x, 32 devices: a whole 2x2x4 slice. The times are simulated.
32 devices in a mesh: grp: 2 (over y), fs: 4 (over z), tp: 4 (over x, core).
Axes of the slice: x: 2, y: 2, z: 4, core: 2. Of those that a mesh axis runs over, the one named last changes fastest.
Arguments:
- tokens: bfloat16 [2560, 2048], P(('grp', 'fs', 'tp')), parts along dimension 0, may hold values from -6 to 6
- mix_gain: bfloat16 [2048], replicated, may hold values from 0.099609375 to 1.8984375
- val_weight: bfloat16 [2048, 1024], P('fs', 'tp'), may hold values from -4 to 4
- gate_weight: bfloat16 [2048, 1024], P('fs', 'tp'), may hold values from -0.125 to 0.125
- conv_taps: bfloat16 [31, 1024], replicated, may hold values from -1 to 1
- chan_gain: bfloat16 [1024], replicated, may hold values from 0.099609375 to 1.8984375
- out_weight: bfloat16 [1024, 2048], P('tp', 'fs'), may hold values from -0.1875 to 0.1875
- mix_post_gain: bfloat16 [2048], replicated, may hold values from 0.099609375 to 1.8984375
- ffn_gain: bfloat16 [2048], replicated, may hold values from 0.099609375 to 1.8984375
- up_gate_weight: bfloat16 [2048, 5120], P('fs', 'tp'), may hold values from -0.125 to 0.125
- up_val_weight: bfloat16 [2048, 5120], P('fs', 'tp'), may hold values from -0.125 to 0.125
- ffn_taps: bfloat16 [2, 3, 5120], replicated, may hold values from -3.5 to 3.5
- down_weight: bfloat16 [5120, 2048], P('tp', 'fs'), may hold values from -0.078125 to 0.078125
- ffn_post_gain: bfloat16 [2048], replicated, may hold values from 0.099609375 to 1.8984375
Outputs:
- layer_out: bfloat16 [2560, 2048], P(('grp', 'fs', 'tp')), parts along dimension 0
There are 2 independent parts, one for each index of `grp`. A program takes and returns all parts, laid end to end along the dimension named above; an argument that names none is the same for every part. Nothing has to cross between parts.
All inputs are finite; a program needn't handle non-finite values.
Results may differ from a plain program's by a relative error of at most 0.019.
Values may be sent and summed in bfloat16 or wider, within the bound.
A program may use at most 64 MiB of HBM per device.

v0:
```python
import jax
import jax.numpy as jnp
from jax import lax
from jax.sharding import PartitionSpec as P

LEN = 64
norm_epsilon = 1e-06
chan_epsilon = 1e-05


def rms_scale(values, gain):
    inverse = lax.rsqrt(jnp.mean(values * values, axis=-1, keepdims=True) + norm_epsilon)
    return values * inverse * gain.astype(jnp.float32)


def depthwise(signal, tap_table):
    taps_count = tap_table.shape[0]
    channels = signal.shape[1]
    shaped = signal.astype(jnp.float32).reshape(signal.shape[0] // LEN, LEN, channels)
    padded = jnp.pad(shaped, ((0, 0), (taps_count - 1, 0), (0, 0)))
    tap_values = tap_table.astype(jnp.float32)
    result = jnp.zeros(shaped.shape, jnp.float32)
    for offset in range(taps_count):
        result = result + padded[:, offset : offset + LEN, :] * tap_values[offset]
    return result.reshape(signal.shape[0], channels)


def make_adder(left, pieces):
    first = jnp.dot(left, pieces[0], preferred_element_type=jnp.float32)
    second = jnp.dot(left, pieces[1], preferred_element_type=jnp.float32)
    return (first, second)


def make_rows_product(left, weight):
    return jnp.dot(left, weight, preferred_element_type=jnp.float32)


def shards(
    tokens,
    mix_gain,
    val_weight,
    gate_weight,
    conv_taps,
    chan_gain,
    out_weight,
    mix_post_gain,
    ffn_gain,
    up_gate_weight,
    up_val_weight,
    ffn_taps,
    down_weight,
    ffn_post_gain,
):
    member = lax.axis_index("tp")
    normed_own = rms_scale(tokens.astype(jnp.float32), mix_gain).astype(jnp.bfloat16)
    normed = lax.all_gather(normed_own, "tp", axis=0, tiled=True)
    local_ch = val_weight.shape[1]
    values, gate_sums = make_adder(
        normed,
        (
            lax.all_gather(val_weight, "fs", axis=0, tiled=True),
            lax.all_gather(gate_weight, "fs", axis=0, tiled=True),
        ),
    )
    glu_out = (values * jax.nn.sigmoid(gate_sums)).astype(jnp.bfloat16)
    own_taps = lax.dynamic_slice_in_dim(conv_taps, member * local_ch, local_ch, 1)
    conv_out = depthwise(glu_out, own_taps)
    totals, squares = lax.psum(
        (jnp.sum(conv_out, axis=1), jnp.sum(conv_out * conv_out, axis=1)), "tp"
    )
    all_channels = chan_gain.shape[0]
    chan_mean = totals[:, None] / all_channels
    chan_var = squares[:, None] / all_channels - chan_mean * chan_mean
    own_gain = lax.dynamic_slice_in_dim(chan_gain, member * local_ch, local_ch, 0).astype(
        jnp.float32
    )
    activated = jax.nn.silu((conv_out - chan_mean) * lax.rsqrt(chan_var + chan_epsilon) * own_gain)
    activated = activated.astype(jnp.bfloat16)
    out_full = lax.all_gather(out_weight, "fs", axis=1, tiled=True)
    mixed_sum = lax.psum_scatter(
        make_rows_product(activated, out_full).astype(jnp.bfloat16),
        "tp",
        scatter_dimension=0,
        tiled=True,
    ).astype(jnp.float32)
    residual = (tokens.astype(jnp.float32) + rms_scale(mixed_sum, mix_post_gain)).astype(
        jnp.bfloat16
    )
    normed_share = rms_scale(residual.astype(jnp.float32), ffn_gain).astype(jnp.bfloat16)
    normed_ffn = lax.all_gather(normed_share, "tp", axis=0, tiled=True)
    local_ff = up_gate_weight.shape[1]
    own_ffn_taps = lax.dynamic_slice_in_dim(ffn_taps, member * local_ff, local_ff, 2)
    gate_full, val_full = (
        lax.all_gather(up_gate_weight, "fs", axis=0, tiled=True),
        lax.all_gather(up_val_weight, "fs", axis=0, tiled=True),
    )
    up_gate = jnp.dot(normed_ffn, gate_full, preferred_element_type=jnp.float32).astype(
        jnp.bfloat16
    )
    up_val = jnp.dot(normed_ffn, val_full, preferred_element_type=jnp.float32).astype(jnp.bfloat16)
    gate_conv = depthwise(up_gate, own_ffn_taps[0])
    val_conv = depthwise(up_val, own_ffn_taps[1])
    hidden = (jax.nn.gelu(gate_conv, approximate=True) * val_conv).astype(jnp.bfloat16)
    down_full = lax.all_gather(down_weight, "fs", axis=1, tiled=True)
    ffn_sum = lax.psum_scatter(
        make_rows_product(hidden, down_full).astype(jnp.bfloat16),
        "tp",
        scatter_dimension=0,
        tiled=True,
    ).astype(jnp.float32)
    return (residual.astype(jnp.float32) + rms_scale(ffn_sum, ffn_post_gain)).astype(jnp.bfloat16)


def solution(mesh):
    return jax.shard_map(
        shards,
        mesh=mesh,
        in_specs=(
            P(("grp", "fs", "tp"), None),
            P(),
            P("fs", "tp"),
            P("fs", "tp"),
            P(),
            P(),
            P("tp", "fs"),
            P(),
            P(),
            P("fs", "tp"),
            P("fs", "tp"),
            P(),
            P("tp", "fs"),
            P(),
        ),
        out_specs=P(("grp", "fs", "tp"), None),
        check_vma=False,
    )
```

profile of v0, /device:TPU:0, one launch (start us, length us, event | category | flops | bytes accessed | tf_op | source)
XLA Modules:
  0.0 503.6 jit_solution(17224619364062690328)
XLA Ops:
  8.0 1.1 fusion.26
  9.1 1.8 fusion.28
  13.9 25.7 %all-gather.11.cloned.1.call-done = bf16[2048,256]{1,0:T(8,128)(2,1)} async-done(((bf16[512,256]{1,0:T(8,128)(2,1)}), bf16[2048,256]{1,0:T(8,128)(2,1)}) %all-gather.11.cloned.1.call-update) | async-done | bytes 1048592 | tf_op jit(solution)/shard_map/all_gather | solution.py:61
  39.7 19.1 %all-gather.9.cloned.1.call-done = bf16[320,2048]{1,0:T(8,128)(2,1)} async-done(((bf16[80,2048]{1,0:T(8,128)(2,1)}), bf16[320,2048]{1,0:T(8,128)(2,1)}) %all-gather.9.cloned.1.call-update) | async-done | bytes 1310736 | tf_op jit(solution)/shard_map/all_gather | solution.py:56
  58.8 2.2 fusion.101
  61.0 27.4 %all-gather.13.cloned.1.call-done = bf16[2048,256]{1,0:T(8,128)(2,1)} async-done(((bf16[512,256]{1,0:T(8,128)(2,1)}), bf16[2048,256]{1,0:T(8,128)(2,1)}) %all-gather.13.cloned.1.call-update) | async-done | bytes 1048592 | tf_op jit(solution)/shard_map/all_gather | solution.py:62
  88.4 1.7 fusion.21
  90.2 1.2 fusion.96
  91.5 6.1 %all-reduce.3 = (f32[320]{0:T(512)S(1)}, f32[320]{0:T(512)S(1)}) all-reduce(f32[320]{0:T(512)S(1)} %reduce_sum.62, f32[320]{0:T(512)S(1)} %reduce_sum.60), channel_id=1, replica_groups=mesh['grp'=2,'fs'=4,'tp'=4] {'tp'}, use_global_device_ids=true, to_apply=%region_4.5 | all-reduce | flops 640 | bytes 5120 | tf_op jit(solution)/shard_map/psum | solution.py:68
  97.8 19.4 %all-gather.15.cloned.1.call-done = bf16[256,2048]{1,0:T(8,128)(2,1)} async-done(((bf16[256,512]{1,0:T(8,128)(2,1)}), bf16[256,2048]{1,0:T(8,128)(2,1)}) %all-gather.15.cloned.1.call-update) | async-done | bytes 1048592 | tf_op jit(solution)/shard_map/all_gather | solution.py:79
  117.2 2.8 convolution_convert_fusion.3
  120.1 25.9 %reduce-scatter.3.cloned.1.call-done = bf16[80,2048]{1,0:T(8,128)(2,1)} async-done(((bf16[320,2048]{1,0:T(8,128)(2,1)}), bf16[80,2048]{1,0:T(8,128)(2,1)}) %reduce-scatter.3.cloned.1.call-update) | async-done | bytes 327696 | tf_op jit(solution)/shard_map/reduce_scatter | solution.py:80
  146.0 1.1 fusion.22
  147.1 1.3 fusion.30
  151.9 15.8 %all-gather.17.cloned.1.call-done = bf16[320,2048]{1,0:T(8,128)(2,1)} async-done(((bf16[80,2048]{1,0:T(8,128)(2,1)}), bf16[320,2048]{1,0:T(8,128)(2,1)}) %all-gather.17.cloned.1.call-update) | async-done | bytes 1310736 | tf_op jit(solution)/shard_map/all_gather | solution.py:90
  167.7 99.6 %all-gather.19.cloned.1.call-done = bf16[2048,1280]{1,0:T(8,128)(2,1)} async-done(((bf16[512,1280]{1,0:T(8,128)(2,1)}), bf16[2048,1280]{1,0:T(8,128)(2,1)}) %all-gather.19.cloned.1.call-update) | async-done | bytes 5242896 | tf_op jit(solution)/shard_map/all_gather | solution.py:94
  267.3 4.8 convolution_convert_fusion.2
  272.2 93.1 %all-gather.21.cloned.1.call-done = bf16[2048,1280]{1,0:T(8,128)(2,1)} async-done(((bf16[512,1280]{1,0:T(8,128)(2,1)}), bf16[2048,1280]{1,0:T(8,128)(2,1)}) %all-gather.21.cloned.1.call-update) | async-done | bytes 5242896 | tf_op jit(solution)/shard_map/all_gather | solution.py:95
  365.3 4.3 convolution_convert_fusion.1
  371.3 92.0 %all-gather.23.cloned.1.call-done = bf16[1280,2048]{1,0:T(8,128)(2,1)} async-done(((bf16[1280,512]{1,0:T(8,128)(2,1)}), bf16[1280,2048]{1,0:T(8,128)(2,1)}) %all-gather.23.cloned.1.call-update) | async-done | bytes 5242896 | tf_op jit(solution)/shard_map/all_gather | solution.py:104
  463.3 5.5 %convolution_convert_fusion = bf16[320,2048]{1,0:T(8,128)(2,1)} fusion(bf16[320,1280]{1,0:T(8,128)(2,1)S(1)} %fusion.16, bf16[1280,2048]{1,0:T(8,128)(2,1)} %all-gather.23.cloned.1.call-done), kind=kOutput, calls=%fused_computation | convolution fusion | flops 1678376960 | bytes 7372800 | tf_op jit(solution)/shard_map/dot_general | solution.py:35
  468.8 24.9 %reduce-scatter.5.cloned.1.call-done = bf16[80,2048]{1,0:T(8,128)(2,1)} async-done(((bf16[320,2048]{1,0:T(8,128)(2,1)}), bf16[80,2048]{1,0:T(8,128)(2,1)}) %reduce-scatter.5.cloned.1.call-update) | async-done | bytes 327696 | tf_op jit(solution)/shard_map/reduce_scatter | solution.py:105
  493.7 1.1 fusion.24
  494.9 1.9 fusion.33
  (59 shorter events, 9.9 us)
Async XLA Ops:
  6.5 33.1 %all-gather.11.cloned.1.call-start = ((), (), s32[]{:S(2)}) async-start(), calls=%async_computation.3 | async-start | bytes 1310720 | tf_op jit(solution)/shard_map/all_gather | solution.py:61
  7.3 51.5 %all-gather.9.cloned.1.call-start = ((), (), s32[]{:S(2)}) async-start(), calls=%async_computation.2 | async-start | bytes 1638400 | tf_op jit(solution)/shard_map/all_gather | solution.py:56
  11.0 77.4 %all-gather.13.cloned.1.call-start = ((), (), s32[]{:S(2)}) async-start(), calls=%async_computation.4 | async-start | bytes 1310720 | tf_op jit(solution)/shard_map/all_gather | solution.py:62
  11.8 105.4 %all-gather.15.cloned.1.call-start = ((), (), s32[]{:S(2)}) async-start(), calls=%async_computation.5 | async-start | bytes 1310720 | tf_op jit(solution)/shard_map/all_gather | solution.py:79
  12.3 133.6 %reduce-scatter.3.cloned.1.call-start = ((), (), s32[]{:S(2)}) async-start(), calls=%async_computation.6 | async-start | bytes 1638400 | tf_op jit(solution)/shard_map/reduce_scatter | solution.py:80
  58.8 29.6 %copy-start.5 = (bf16[320,2048]{1,0:T(8,128)(2,1)S(1)}, bf16[320,2048]{1,0:T(8,128)(2,1)}, u32[]{:S(2)}) copy-start(bf16[320,2048]{1,0:T(8,128)(2,1)} %all-gather.9.cloned.1.call-done) | copy-start | bytes 3932164
  97.8 22.3 %copy-start.2 = (bf16[2048]{0:T(1024)(128)(2,1)S(1)}, bf16[2048]{0:T(1024)(128)(2,1)}, u32[]{:S(2)}) copy-start(bf16[2048]{0:T(1024)(128)(2,1)} %param.21) | copy-start | bytes 12292
  97.8 22.3 %copy-start.3 = (bf16[2048]{0:T(1024)(128)(2,1)S(1)}, bf16[2048]{0:T(1024)(128)(2,1)}, u32[]{:S(2)}) copy-start(bf16[2048]{0:T(1024)(128)(2,1)} %param.22) | copy-start | bytes 12292
  97.8 49.3 %copy-start = (bf16[80,2048]{1,0:T(8,128)(2,1)S(1)}, bf16[80,2048]{1,0:T(8,128)(2,1)}, u32[]{:S(2)}) copy-start(bf16[80,2048]{1,0:T(8,128)(2,1)} %param.14) | copy-start | bytes 983044
  120.0 47.7 %all-gather.17.cloned.1.call-start = ((), (), s32[]{:S(2)}) async-start(), calls=%async_computation.7 | async-start | bytes 1638400 | tf_op jit(solution)/shard_map/all_gather | solution.py:90
  149.4 118.0 %all-gather.19.cloned.1.call-start = ((), (), s32[]{:S(2)}) async-start(), calls=%async_computation.8 | async-start | bytes 6553600 | tf_op jit(solution)/shard_map/all_gather | solution.py:94
  150.1 1.5 copy-start.1
  150.1 215.2 %all-gather.21.cloned.1.call-start = ((), (), s32[]{:S(2)}) async-start(), calls=%async_computation.9 | async-start | bytes 6553600 | tf_op jit(solution)/shard_map/all_gather | solution.py:95
  150.9 312.4 %all-gather.23.cloned.1.call-start = ((), (), s32[]{:S(2)}) async-start(), calls=%async_computation.10 | async-start | bytes 6553600 | tf_op jit(solution)/shard_map/all_gather | solution.py:104
  151.6 342.1 %reduce-scatter.5.cloned.1.call-start = ((), (), s32[]{:S(2)}) async-start(), calls=%async_computation.11 | async-start | bytes 1638400 | tf_op jit(solution)/shard_map/reduce_scatter | solution.py:105
  272.1 93.2 %copy-start.6 = (bf16[320,2048]{1,0:T(8,128)(2,1)S(1)}, bf16[320,2048]{1,0:T(8,128)(2,1)}, u32[]{:S(2)}) copy-start(bf16[320,2048]{1,0:T(8,128)(2,1)} %all-gather.17.cloned.1.call-done) | copy-start | bytes 3932164
  371.3 97.5 %copy-start.4 = (bf16[2048]{0:T(1024)(128)(2,1)S(1)}, bf16[2048]{0:T(1024)(128)(2,1)}, u32[]{:S(2)}) copy-start(bf16[2048]{0:T(1024)(128)(2,1)} %param.27) | copy-start | bytes 12292
Sparse Core Ops, SparseCore 0:
  8.9 30.7 all-gather.10
  41.2 17.5 all-gather.8
  60.4 27.9 all-gather.12
  89.8 27.3 all-gather.14
  120.1 25.7 reduce-scatter.2
  149.5 18.1 all-gather.16
  169.3 98.0 all-gather.18
  268.9 96.3 all-gather.20
  366.9 96.3 all-gather.22
  468.9 24.7 reduce-scatter.4
where the time goes:
time: 504 us
  waiting for transfers between devices  447 us (89%)
  matrix products  21.4 us (4%)
  other arithmetic  14.9 us (3%)
  between operations  13.8 us (3%)
  blocking collectives  6.05 us (1%)
    all_gather x1, waiting for transfers between devices, shards(): lax.all_gather(up_gate_weight, 'fs', axis=0, tiled=True)  99.6 us
    all_gather x1, waiting for transfers between devices, shards(): lax.all_gather(up_val_weight, 'fs', axis=0, tiled=True)  93.1 us
    all_gather x1, waiting for transfers between devices, shards(): down_full = lax.all_gather(down_weight, 'fs', axis=1, tiled=True)  92 us
    all_gather x1, waiting for transfers between devices, shards(): lax.all_gather(gate_weight, 'fs', axis=0, tiled=True)  27.4 us
    reduce_scatter x1, waiting for transfers between devices, shards(): lax.psum_scatter(make_rows_product(activated, out_full).astype(jnp.bfloat...  25.9 us
    all_gather x1, waiting for transfers between devices, shards(): lax.all_gather(val_weight, 'fs', axis=0, tiled=True)  25.7 us
    reduce_scatter x1, waiting for transfers between devices, shards(): lax.psum_scatter(make_rows_product(hidden, down_full).astype(jnp.bfloat16...  24.9 us
    all_gather x1, waiting for transfers between devices, shards(): out_full = lax.all_gather(out_weight, 'fs', axis=1, tiled=True)  19.4 us
  transfers between devices with their start and end apart: 10, of which 10 were waited for; matrix products, arithmetic and copies ran while one was open for 4% of the time, Pallas kernels for 0%

commit v1 on v0

--- a/solution.py
+++ b/solution.py
@@ -101,7 +101,7 @@
     gate_conv = depthwise(up_gate, own_ffn_taps[0])
     val_conv = depthwise(up_val, own_ffn_taps[1])
     hidden = (jax.nn.gelu(gate_conv, approximate=True) * val_conv).astype(jnp.bfloat16)
-    down_full = lax.all_gather(down_weight, "fs", axis=1, tiled=True)
+    down_full = jnp.concatenate(lax.all_gather(down_weight, "fs"), axis=1)
     ffn_sum = lax.psum_scatter(
         make_rows_product(hidden, down_full).astype(jnp.bfloat16),
         "tp",

time: 504 us -> 514 us (1.020)
  local copies, waits for them, and re-layouts: 0.3 us -> 8.87 us
    reshape x0 -> x1, local copies, waits for them, and re-layouts: none -> 7.86 us  [shards(): down_full = jnp.concatenate(lax.all_gather(down_weight, 'fs'), axis=1)]
where the time goes in v1:
time: 514 us
  waiting for transfers between devices  448 us (87%)
  matrix products  21.3 us (4%)
  other arithmetic  14.8 us (3%)
  between operations  13.8 us (3%)
  local copies, waits for them, and re-layouts  8.87 us (2%)
  blocking collectives  6.05 us (1%)
    all_gather x1, waiting for transfers between devices, shards(): lax.all_gather(up_gate_weight, 'fs', axis=0, tiled=True)  99.6 us
    all_gather x1, waiting for transfers between devices, shards(): down_full = jnp.concatenate(lax.all_gather(down_weight, 'fs'), axis=1)  93.5 us
    all_gather x1, waiting for transfers between devices, shards(): lax.all_gather(up_val_weight, 'fs', axis=0, tiled=True)  93.1 us
    all_gather x1, waiting for transfers between devices, shards(): lax.all_gather(gate_weight, 'fs', axis=0, tiled=True)  27.4 us
    reduce_scatter x1, waiting for transfers between devices, shards(): lax.psum_scatter(make_rows_product(activated, out_full).astype(jnp.bfloat...  25.9 us
    all_gather x1, waiting for transfers between devices, shards(): lax.all_gather(val_weight, 'fs', axis=0, tiled=True)  25.7 us
    reduce_scatter x1, waiting for transfers between devices, shards(): lax.psum_scatter(make_rows_product(hidden, down_full).astype(jnp.bfloat16...  24.9 us
    all_gather x1, waiting for transfers between devices, shards(): out_full = lax.all_gather(out_weight, 'fs', axis=1, tiled=True)  19.4 us
  transfers between devices with their start and end apart: 10, of which 10 were waited for; matrix products, arithmetic and copies ran while one was open for 4% of the time, Pallas kernels for 0%

profile of v1, /device:TPU:0, one launch (start us, length us, event | category | flops | bytes accessed | tf_op | source)
XLA Modules:
  0.0 513.7 jit_solution(4863321637175996717)
XLA Ops:
  8.0 1.1 fusion.26
  9.1 1.8 fusion.28
  13.9 25.7 %all-gather.12.cloned.1.call-done = bf16[2048,256]{1,0:T(8,128)(2,1)} async-done(((bf16[512,256]{1,0:T(8,128)(2,1)}), bf16[2048,256]{1,0:T(8,128)(2,1)}) %all-gather.12.cloned.1.call-update) | async-done | bytes 1048592 | tf_op jit(solution)/shard_map/all_gather | solution.py:61
  39.7 19.1 %all-gather.10.cloned.1.call-done = bf16[320,2048]{1,0:T(8,128)(2,1)} async-done(((bf16[80,2048]{1,0:T(8,128)(2,1)}), bf16[320,2048]{1,0:T(8,128)(2,1)}) %all-gather.10.cloned.1.call-update) | async-done | bytes 1310736 | tf_op jit(solution)/shard_map/all_gather | solution.py:56
  58.8 2.2 fusion.101
  61.0 27.4 %all-gather.14.cloned.1.call-done = bf16[2048,256]{1,0:T(8,128)(2,1)} async-done(((bf16[512,256]{1,0:T(8,128)(2,1)}), bf16[2048,256]{1,0:T(8,128)(2,1)}) %all-gather.14.cloned.1.call-update) | async-done | bytes 1048592 | tf_op jit(solution)/shard_map/all_gather | solution.py:62
  88.4 1.8 fusion.21
  90.2 1.2 fusion.96
  91.5 6.1 %all-reduce.3 = (f32[320]{0:T(512)S(1)}, f32[320]{0:T(512)S(1)}) all-reduce(f32[320]{0:T(512)S(1)} %reduce_sum.62, f32[320]{0:T(512)S(1)} %reduce_sum.60), channel_id=1, replica_groups=mesh['grp'=2,'fs'=4,'tp'=4] {'tp'}, use_global_device_ids=true, to_apply=%region_4.5 | all-reduce | flops 640 | bytes 5120 | tf_op jit(solution)/shard_map/psum | solution.py:68
  97.8 19.4 %all-gather.16.cloned.1.call-done = bf16[256,2048]{1,0:T(8,128)(2,1)} async-done(((bf16[256,512]{1,0:T(8,128)(2,1)}), bf16[256,2048]{1,0:T(8,128)(2,1)}) %all-gather.16.cloned.1.call-update) | async-done | bytes 1048592 | tf_op jit(solution)/shard_map/all_gather | solution.py:79
  117.2 2.8 convolution_convert_fusion.3
  120.1 25.9 %reduce-scatter.3.cloned.1.call-done = bf16[80,2048]{1,0:T(8,128)(2,1)} async-done(((bf16[320,2048]{1,0:T(8,128)(2,1)}), bf16[80,2048]{1,0:T(8,128)(2,1)}) %reduce-scatter.3.cloned.1.call-update) | async-done | bytes 327696 | tf_op jit(solution)/shard_map/reduce_scatter | solution.py:80
  147.1 1.3 fusion.30
  152.6 15.8 %all-gather.18.cloned.1.call-done = bf16[320,2048]{1,0:T(8,128)(2,1)} async-done(((bf16[80,2048]{1,0:T(8,128)(2,1)}), bf16[320,2048]{1,0:T(8,128)(2,1)}) %all-gather.18.cloned.1.call-update) | async-done | bytes 1310736 | tf_op jit(solution)/shard_map/all_gather | solution.py:90
  168.4 99.6 %all-gather.20.cloned.1.call-done = bf16[2048,1280]{1,0:T(8,128)(2,1)} async-done(((bf16[512,1280]{1,0:T(8,128)(2,1)}), bf16[2048,1280]{1,0:T(8,128)(2,1)}) %all-gather.20.cloned.1.call-update) | async-done | bytes 5242896 | tf_op jit(solution)/shard_map/all_gather | solution.py:94
  268.0 4.7 convolution_convert_fusion.2
  272.9 93.1 %all-gather.22.cloned.1.call-done = bf16[2048,1280]{1,0:T(8,128)(2,1)} async-done(((bf16[512,1280]{1,0:T(8,128)(2,1)}), bf16[2048,1280]{1,0:T(8,128)(2,1)}) %all-gather.22.cloned.1.call-update) | async-done | bytes 5242896 | tf_op jit(solution)/shard_map/all_gather | solution.py:95
  366.0 4.3 convolution_convert_fusion.1
  370.5 93.5 %all-gather.24.cloned.1.call-done = bf16[5120,512]{1,0:T(8,128)(2,1)} async-done(((bf16[1280,512]{1,0:T(8,128)(2,1)}), bf16[5120,512]{1,0:T(8,128)(2,1)}) %all-gather.24.cloned.1.call-update) | async-done | bytes 5242896 | tf_op jit(solution)/shard_map/all_gather | solution.py:104
  464.0 7.9 %copy.15 = bf16[1280,4,512]{0,2,1:T(8,128)(2,1)} copy(bf16[1280,4,512]{2,0,1:T(8,128)(2,1)} %bitcast.62) | data formatting | bytes 10485760 | tf_op jit(solution)/shard_map/reshape | solution.py:104
  471.9 1.5 fusion.8
  473.4 5.4 %convolution_convert_fusion = bf16[320,2048]{1,0:T(8,128)(2,1)} fusion(bf16[320,1280]{1,0:T(8,128)(2,1)S(1)} %bitcast.66, bf16[1280,2048]{0,1:T(8,128)(2,1)} %bitcast.63), kind=kOutput, calls=%fused_computation | convolution fusion | flops 1678376960 | bytes 7372800 | tf_op jit(solution)/shard_map/dot_general | solution.py:35
  478.9 24.9 %reduce-scatter.5.cloned.1.call-done = bf16[80,2048]{1,0:T(8,128)(2,1)} async-done(((bf16[320,2048]{1,0:T(8,128)(2,1)}), bf16[80,2048]{1,0:T(8,128)(2,1)}) %reduce-scatter.5.cloned.1.call-update) | async-done | bytes 327696 | tf_op jit(solution)/shard_map/reduce_scatter | solution.py:105
  504.9 1.9 fusion.33
  (62 shorter events, 11.4 us)
Async XLA Ops:
  6.5 33.1 %all-gather.12.cloned.1.call-start = ((), (), s32[]{:S(2)}) async-start(), calls=%async_computation.3 | async-start | bytes 1310720 | tf_op jit(solution)/shard_map/all_gather | solution.py:61
  7.3 51.5 %all-gather.10.cloned.1.call-start = ((), (), s32[]{:S(2)}) async-start(), calls=%async_computation.2 | async-start | bytes 1638400 | tf_op jit(solution)/shard_map/all_gather | solution.py:56
  11.0 77.4 %all-gather.14.cloned.1.call-start = ((), (), s32[]{:S(2)}) async-start(), calls=%async_computation.4 | async-start | bytes 1310720 | tf_op jit(solution)/shard_map/all_gather | solution.py:62
  11.8 105.4 %all-gather.16.cloned.1.call-start = ((), (), s32[]{:S(2)}) async-start(), calls=%async_computation.5 | async-start | bytes 1310720 | tf_op jit(solution)/shard_map/all_gather | solution.py:79
  12.3 133.6 %reduce-scatter.3.cloned.1.call-start = ((), (), s32[]{:S(2)}) async-start(), calls=%async_computation.6 | async-start | bytes 1638400 | tf_op jit(solution)/shard_map/reduce_scatter | solution.py:80
  58.8 29.6 %copy-start.7 = (bf16[320,2048]{1,0:T(8,128)(2,1)S(1)}, bf16[320,2048]{1,0:T(8,128)(2,1)}, u32[]{:S(2)}) copy-start(bf16[320,2048]{1,0:T(8,128)(2,1)} %all-gather.10.cloned.1.call-done) | copy-start | bytes 3932164
  97.8 22.3 %copy-start.4 = (bf16[2048]{0:T(1024)(128)(2,1)S(1)}, bf16[2048]{0:T(1024)(128)(2,1)}, u32[]{:S(2)}) copy-start(bf16[2048]{0:T(1024)(128)(2,1)} %param.21) | copy-start | bytes 12292
  97.8 22.3 %copy-start.5 = (bf16[2048]{0:T(1024)(128)(2,1)S(1)}, bf16[2048]{0:T(1024)(128)(2,1)}, u32[]{:S(2)}) copy-start(bf16[2048]{0:T(1024)(128)(2,1)} %param.22) | copy-start | bytes 12292
  97.8 49.3 %copy-start.2 = (bf16[80,2048]{1,0:T(8,128)(2,1)S(1)}, bf16[80,2048]{1,0:T(8,128)(2,1)}, u32[]{:S(2)}) copy-start(bf16[80,2048]{1,0:T(8,128)(2,1)} %param.14) | copy-start | bytes 983044
  120.0 48.4 %all-gather.18.cloned.1.call-start = ((), (), s32[]{:S(2)}) async-start(), calls=%async_computation.7 | async-start | bytes 1638400 | tf_op jit(solution)/shard_map/all_gather | solution.py:90
  148.5 0.7 copy-start
  150.1 118.0 %all-gather.20.cloned.1.call-start = ((), (), s32[]{:S(2)}) async-start(), calls=%async_computation.8 | async-start | bytes 6553600 | tf_op jit(solution)/shard_map/all_gather | solution.py:94
  150.8 1.5 copy-start.3
  150.8 215.2 %all-gather.22.cloned.1.call-start = ((), (), s32[]{:S(2)}) async-start(), calls=%async_computation.9 | async-start | bytes 6553600 | tf_op jit(solution)/shard_map/all_gather | solution.py:95
  151.6 312.4 %all-gather.24.cloned.1.call-start = ((), (), s32[]{:S(2)}) async-start(), calls=%async_computation.11 | async-start | bytes 6553600 | tf_op jit(solution)/shard_map/all_gather | solution.py:104
  152.3 351.5 %reduce-scatter.5.cloned.1.call-start = ((), (), s32[]{:S(2)}) async-start(), calls=%async_computation.10 | async-start | bytes 1638400 | tf_op jit(solution)/shard_map/reduce_scatter | solution.py:105
  272.8 93.2 %copy-start.8 = (bf16[320,2048]{1,0:T(8,128)(2,1)S(1)}, bf16[320,2048]{1,0:T(8,128)(2,1)}, u32[]{:S(2)}) copy-start(bf16[320,2048]{1,0:T(8,128)(2,1)} %all-gather.18.cloned.1.call-done) | copy-start | bytes 3932164
  473.4 5.5 %copy-start.6 = (bf16[2048]{0:T(1024)(128)(2,1)S(1)}, bf16[2048]{0:T(1024)(128)(2,1)}, u32[]{:S(2)}) copy-start(bf16[2048]{0:T(1024)(128)(2,1)} %param.27) | copy-start | bytes 12292
  478.8 26.1 %copy-start.1 = (bf16[80,2048]{1,0:T(8,128)(2,1)S(1)}, bf16[80,2048]{1,0:T(8,128)(2,1)}, u32[]{:S(2)}) copy-start(bf16[80,2048]{1,0:T(8,128)(2,1)} %copy-done) | copy-start | bytes 983044
Sparse Core Ops, SparseCore 0:
  8.9 30.7 all-gather.11
  41.2 17.5 all-gather.9
  60.4 27.9 all-gather.13
  89.8 27.3 all-gather.15
  120.1 25.7 reduce-scatter.2
  150.2 18.1 all-gather.17
  170.0 98.0 all-gather.19
  269.6 96.3 all-gather.21
  367.6 96.3 all-gather.23
  479.0 24.7 reduce-scatter.4
